TPU v7x, 32 devices: a whole 2x2x4 slice. The times are simulated.
32 devices in a mesh: fs: 8 (over z, y), tp: 4 (over x, core).
Axes of the slice: x: 2, y: 2, z: 4, core: 2. Of those that a mesh axis runs over, the one named last changes fastest.
Arguments:
- tokens: bfloat16 [4096, 2048], P(('fs', 'tp')), may hold values from -6 to 6
- gate_proj: bfloat16 [2048, 512], P('fs', 'tp'), may hold values from -0.125 to 0.125
- signal_proj: bfloat16 [2048, 512], P('fs', 'tp'), may hold values from -1.5467961 to 1.5467961
- spatial: bfloat16 [4, 128, 128], replicated, may hold values from -0.5 to 0.5
- signal_gain: bfloat16 [512], P('tp'), may hold values from 0.099609375 to 1.8984375
- mixer_out: bfloat16 [512, 2048], P('tp', 'fs'), may hold values from -0.25 to 0.25
- mixer_gain: bfloat16 [2048], replicated, may hold values from 0.099609375 to 1.8984375
- ffn_gate: bfloat16 [2048, 5632], P('fs', 'tp'), may hold values from -0.125 to 0.125
- ffn_value: bfloat16 [2048, 5632], P('fs', 'tp'), may hold values from -0.125 to 0.125
- conv_taps: bfloat16 [3, 5632], P(None, 'tp'), may hold values from -3.5 to 3.5
- ffn_down: bfloat16 [5632, 2048], P('tp', 'fs'), may hold values from -0.078125 to 0.078125
- output_gain: bfloat16 [2048], replicated, may hold values from 0.099609375 to 1.8984375
Outputs:
- result: bfloat16 [4096, 2048], P(('fs', 'tp'))
All inputs are finite; a program needn't handle non-finite values.
Results may differ from a plain program's by a relative error of at most 0.01.
Values may be sent and summed in bfloat16 or wider, within the bound.
A program may use at most 64 MiB of HBM per device.

v0:
```python
import math
import jax
import jax.numpy as jnp
from jax import lax
from jax.sharding import PartitionSpec as P

MIX_WIDTH = 512
HEAD_SIZE = 128
BLOCK = 128
SEGMENT = 64
EPSILON = 1e-05
RESIDUAL_SCALE = math.sqrt(2.0)


def normalize(values):
    row_mean = jnp.mean(values, axis=-1, keepdims=True)
    centred = values - row_mean
    spread = jnp.mean(centred * centred, axis=-1, keepdims=True)
    return centred * lax.rsqrt(spread + EPSILON)


def causal_conv(gate_pre, conv_taps):
    taps = conv_taps.astype(jnp.float32)
    width = gate_pre.shape[1]
    shifted_one = jnp.concatenate([jnp.zeros((1, width), jnp.float32), gate_pre[:-1]], axis=0)
    shifted_two = jnp.concatenate([jnp.zeros((2, width), jnp.float32), gate_pre[:-2]], axis=0)
    return taps[0] * shifted_two + taps[1] * shifted_one + taps[2] * gate_pre


def shards(
    tokens,
    gate_proj,
    signal_proj,
    spatial,
    signal_gain,
    mixer_out,
    mixer_gain,
    ffn_gate,
    ffn_value,
    conv_taps,
    ffn_down,
    output_gain,
):
    residual = tokens.astype(jnp.float32)
    mix_input = normalize(residual).astype(jnp.bfloat16)
    segment_ids = jnp.arange(BLOCK) // SEGMENT
    allowed = segment_ids[None, :] <= segment_ids[:, None]
    masked = jnp.where(allowed[None], spatial, jnp.zeros_like(spatial))
    group_input = lax.all_gather(mix_input, "tp", axis=0, tiled=True)
    group_rows = group_input.shape[0]
    column_count = gate_proj.shape[1]
    pieces = (
        lax.all_gather(gate_proj, "fs", axis=0, tiled=True),
        lax.all_gather(signal_proj, "fs", axis=0, tiled=True),
    )
    left_part = group_input
    gate_sum = jnp.dot(left_part, pieces[0], preferred_element_type=jnp.float32)
    signal_sum = jnp.dot(left_part, pieces[1], preferred_element_type=jnp.float32)
    branch_gate = jax.nn.gelu(gate_sum)
    branch_signal = jax.nn.gelu(signal_sum)
    total_sum, square_sum = lax.psum(
        (jnp.sum(branch_signal, axis=1), jnp.sum(branch_signal * branch_signal, axis=1)), "tp"
    )
    row_mean = total_sum / MIX_WIDTH
    spread = square_sum / MIX_WIDTH - row_mean * row_mean
    spatial_input = (
        (branch_signal - row_mean[:, None])
        * lax.rsqrt(spread[:, None] + EPSILON)
        * signal_gain.astype(jnp.float32)
    ).astype(jnp.bfloat16)
    head_index = lax.axis_index("tp") * column_count // HEAD_SIZE
    own_weights = lax.dynamic_index_in_dim(masked, head_index, 0, keepdims=False)
    blocks = spatial_input.reshape(group_rows // BLOCK, BLOCK, column_count)
    mixed_rows = jnp.einsum(
        "ij,njc->nic", own_weights, blocks, preferred_element_type=jnp.float32
    ).reshape(group_rows, column_count)
    gated_rows = (branch_gate * mixed_rows).astype(jnp.bfloat16)
    out_columns = lax.all_gather(mixer_out, "fs", axis=1, tiled=True)
    selected = gated_rows
    mix_out = lax.psum_scatter(
        jnp.dot(selected, out_columns, preferred_element_type=jnp.float32).astype(jnp.bfloat16),
        "tp",
        scatter_dimension=0,
        tiled=True,
    ).astype(jnp.float32)
    middle = (
        normalize(RESIDUAL_SCALE * residual + mix_out) * mixer_gain.astype(jnp.float32)
    ).astype(jnp.bfloat16)
    middle_wide = middle.astype(jnp.float32)
    ffn_input = normalize(middle_wide).astype(jnp.bfloat16)
    group_ffn = lax.all_gather(ffn_input, "tp", axis=0, tiled=True)
    pieces = (
        lax.all_gather(ffn_gate, "fs", axis=0, tiled=True),
        lax.all_gather(ffn_value, "fs", axis=0, tiled=True),
    )
    left_part = group_ffn
    gate_pre = jnp.dot(left_part, pieces[0], preferred_element_type=jnp.float32)
    value_pre = jnp.dot(left_part, pieces[1], preferred_element_type=jnp.float32)
    whole_down = lax.all_gather(ffn_down, "fs", axis=1, tiled=True)
    hidden = (jax.nn.silu(causal_conv(gate_pre, conv_taps)) * value_pre).astype(jnp.bfloat16)
    selected = hidden
    ffn_out = lax.psum_scatter(
        jnp.dot(selected, whole_down, preferred_element_type=jnp.float32).astype(jnp.bfloat16),
        "tp",
        scatter_dimension=0,
        tiled=True,
    ).astype(jnp.float32)
    return (
        normalize(RESIDUAL_SCALE * middle_wide + ffn_out) * output_gain.astype(jnp.float32)
    ).astype(jnp.bfloat16)


def solution(mesh):
    in_specs = (
        P(("fs", "tp"), None),
        P("fs", "tp"),
        P("fs", "tp"),
        P(),
        P("tp"),
        P("tp", "fs"),
        P(),
        P("fs", "tp"),
        P("fs", "tp"),
        P(None, "tp"),
        P("tp", "fs"),
        P(),
    )
    out_specs = P(("fs", "tp"), None)
    return jax.shard_map(shards, mesh=mesh, in_specs=in_specs, out_specs=out_specs, check_vma=False)
```

profile of v0, /device:TPU:0, one launch (start us, length us, event | category | flops | bytes accessed | tf_op | source)
XLA Modules:
  0.0 485.2 jit_solution(16382907867453121920)
XLA Ops:
  7.4 1.2 convert_reduce_fusion.1
  8.6 1.3 fusion.7
  9.9 2.2 fusion.8
  12.2 0.7 convert_element_type.53
  13.0 33.3 %all_gather.26 = bf16[2048,128]{1,0:T(8,128)(2,1)S(1)} all-gather(bf16[256,128]{1,0:T(8,128)(2,1)} %param.14), channel_id=1, replica_groups=mesh['fs'=8,'tp'=4] {'fs'}, dimensions={0}, use_global_device_ids=true | all-gather | bytes 589824 | tf_op jit(solution)/shard_map/all_gather | solution.py:54
  46.3 31.5 %all_gather.25 = bf16[2048,128]{1,0:T(8,128)(2,1)S(1)} all-gather(bf16[256,128]{1,0:T(8,128)(2,1)S(1)} %copy-done.1), channel_id=1, replica_groups=mesh['fs'=8,'tp'=4] {'fs'}, dimensions={0}, use_global_device_ids=true | all-gather | bytes 589824 | tf_op jit(solution)/shard_map/all_gather | solution.py:53
  77.8 31.2 %all_gather.27 = bf16[128,2048]{1,0:T(8,128)(2,1)S(1)} all-gather(bf16[128,256]{1,0:T(8,128)(2,1)S(1)} %copy-done.2), channel_id=1, replica_groups=mesh['fs'=8,'tp'=4] {'fs'}, dimensions={1}, use_global_device_ids=true | all-gather | bytes 589824 | tf_op jit(solution)/shard_map/all_gather | solution.py:78
  109.0 2.4 fusion.38
  111.4 5.7 %all-reduce.2 = (f32[512]{0:T(512)S(1)}, f32[512]{0:T(512)S(1)}) all-reduce(f32[512]{0:T(512)S(1)} %get-tuple-element.6, f32[512]{0:T(512)S(1)} %get-tuple-element.5), channel_id=1, replica_groups=mesh['fs'=8,'tp'=4] {'tp'}, use_global_device_ids=true, to_apply=%region_5.6 | all-reduce | flops 1024 | bytes 8192 | tf_op jit(solution)/shard_map/psum | solution.py:61
  117.3 0.9 fusion.30
  118.2 2.3 fusion.21
  120.6 2.0 convolution_convert_fusion
  122.7 0.5 all-gather.10.cloned.1.call-update
  123.3 31.8 %reduce-scatter.3.cloned.1.call-done = bf16[128,2048]{1,0:T(8,128)(2,1)} async-done(((bf16[512,2048]{1,0:T(8,128)(2,1)}), bf16[128,2048]{1,0:T(8,128)(2,1)}) %reduce-scatter.3.cloned.1.call-update) | async-done | bytes 524304 | tf_op jit(solution)/shard_map/reduce_scatter | solution.py:80
  155.1 1.3 fusion.12
  156.4 1.4 multiply_reduce_fusion.1
  157.8 1.4 convert_reduce_fusion
  159.3 0.3 fusion.5
  159.6 1.1 fusion.6
  160.7 0.5 all-gather.12.cloned.1.call-update
  161.3 0.7 all-gather.14.cloned.1.call-update
  162.0 0.2 reduce-scatter.5.cloned.1.call-start
  162.3 56.3 %all-gather.10.cloned.1.call-done = bf16[2048,1408]{1,0:T(8,128)(2,1)} async-done(((bf16[256,1408]{1,0:T(8,128)(2,1)}), bf16[2048,1408]{1,0:T(8,128)(2,1)}) %all-gather.10.cloned.1.call-update) | async-done | bytes 5767184 | tf_op jit(solution)/shard_map/all_gather | solution.py:93
  218.6 22.0 %all-gather.8.cloned.1.call-done = bf16[512,2048]{1,0:T(8,128)(2,1)} async-done(((bf16[128,2048]{1,0:T(8,128)(2,1)}), bf16[512,2048]{1,0:T(8,128)(2,1)}) %all-gather.8.cloned.1.call-update) | async-done | bytes 2097168 | tf_op jit(solution)/shard_map/all_gather | solution.py:91
  240.6 8.4 %fusion.39 = f32[512,1408]{1,0:T(8,128)} fusion(bf16[512,2048]{1,0:T(8,128)(2,1)} %all-gather.8.cloned.1.call-done, bf16[2048,1408]{1,0:T(8,128)(2,1)} %all-gather.10.cloned.1.call-done), kind=kOutput, calls=%fused_computation.74 | convolution fusion | flops 2952790016 | bytes 10747904 | tf_op jit(solution)/shard_map/dot_general | solution.py:97
  249.0 85.8 %all-gather.12.cloned.1.call-done = bf16[2048,1408]{1,0:T(8,128)(2,1)} async-done(((bf16[256,1408]{1,0:T(8,128)(2,1)}), bf16[2048,1408]{1,0:T(8,128)(2,1)}) %all-gather.12.cloned.1.call-update) | async-done | bytes 5767184 | tf_op jit(solution)/shard_map/all_gather | solution.py:94
  334.8 93.1 %all-gather.14.cloned.1.call-done = bf16[1408,2048]{1,0:T(8,128)(2,1)} async-done(((bf16[1408,256]{1,0:T(8,128)(2,1)}), bf16[1408,2048]{1,0:T(8,128)(2,1)}) %all-gather.14.cloned.1.call-update) | async-done | bytes 5767184 | tf_op jit(solution)/shard_map/all_gather | solution.py:99
  428.0 15.5 %convolution_convert_fusion.1 = bf16[512,2048]{1,0:T(8,128)(2,1)} fusion(bf16[1408,2048]{1,0:T(8,128)(2,1)} %all-gather.14.cloned.1.call-done, bf16[512,2048]{1,0:T(8,128)(2,1)S(1)} %copy-done.6, bf16[2048,1408]{1,0:T(8,128)(2,1)} %all-gather.12.cloned.1.call-done, f32[512,1408]{1,0:T(8,128)} %fusion.39, f32[511,1408]{1,0:T(8,128)} %bitcast.24, ...), kind=kOutput, calls=%fused_computation.3 | convolution fusion | flops 5914558464 | bytes 24379392 | tf_op jit(solution)/shard_map/dot_general | solution.py:103
  443.6 29.5 %reduce-scatter.5.cloned.1.call-done = bf16[128,2048]{1,0:T(8,128)(2,1)} async-done(((bf16[512,2048]{1,0:T(8,128)(2,1)}), bf16[128,2048]{1,0:T(8,128)(2,1)}) %reduce-scatter.5.cloned.1.call-update) | async-done | bytes 524304 | tf_op jit(solution)/shard_map/reduce_scatter | solution.py:102
  473.0 1.3 fusion.11
  474.3 1.4 multiply_reduce_fusion
  475.7 2.1 multiply_convert_fusion
  (41 shorter events, 0.7 us)
Async XLA Ops:
  7.4 38.9 %copy-start.1 = (bf16[256,128]{1,0:T(8,128)(2,1)S(1)}, bf16[256,128]{1,0:T(8,128)(2,1)}, u32[]{:S(2)}) copy-start(bf16[256,128]{1,0:T(8,128)(2,1)} %param.13) | copy-start | bytes 196612
  7.4 70.4 %copy-start.2 = (bf16[128,256]{1,0:T(8,128)(2,1)S(1)}, bf16[128,256]{1,0:T(8,128)(2,1)}, u32[]{:S(2)}) copy-start(bf16[128,256]{1,0:T(8,128)(2,1)} %param.17) | copy-start | bytes 196612
  7.4 101.6 %all-gather.6.cloned.1.call-start = ((), (), s32[]{:S(2)}) async-start(), calls=%async_computation.2 | async-start | bytes 2621440 | tf_op jit(solution)/shard_map/all_gather | solution.py:49
  12.1 143.0 %reduce-scatter.3.cloned.1.call-start = ((), (), s32[]{:S(2)}) async-start(), calls=%async_computation.3 | async-start | bytes 2621440 | tf_op jit(solution)/shard_map/reduce_scatter | solution.py:80
  120.6 2.7 copy-start.4
  120.6 34.5 %copy-start = (bf16[128,2048]{1,0:T(8,128)(2,1)S(1)}, bf16[128,2048]{1,0:T(8,128)(2,1)}, u32[]{:S(2)}) copy-start(bf16[128,2048]{1,0:T(8,128)(2,1)} %param.12) | copy-start | bytes 1572868
  122.6 96.0 %all-gather.10.cloned.1.call-start = ((), (), s32[]{:S(2)}) async-start(), calls=%async_computation.5 | async-start | bytes 6488064 | tf_op jit(solution)/shard_map/all_gather | solution.py:93
  123.2 117.4 %all-gather.8.cloned.1.call-start = ((), (), s32[]{:S(2)}) async-start(), calls=%async_computation.4 | async-start | bytes 2621440 | tf_op jit(solution)/shard_map/all_gather | solution.py:91
  156.4 5.8 %copy-start.3 = (bf16[3,1408]{1,0:T(4,128)(2,1)S(1)}, bf16[3,1408]{1,0:T(4,128)(2,1)}, u32[]{:S(2)}) copy-start(bf16[3,1408]{1,0:T(4,128)(2,1)} %param.21) | copy-start | bytes 25348
  160.7 174.2 %all-gather.12.cloned.1.call-start = ((), (), s32[]{:S(2)}) async-start(), calls=%async_computation.6 | async-start | bytes 6488064 | tf_op jit(solution)/shard_map/all_gather | solution.py:94
  161.3 266.7 %all-gather.14.cloned.1.call-start = ((), (), s32[]{:S(2)}) async-start(), calls=%async_computation.7 | async-start | bytes 6488064 | tf_op jit(solution)/shard_map/all_gather | solution.py:99
  162.0 311.0 %reduce-scatter.5.cloned.1.call-start = ((), (), s32[]{:S(2)}) async-start(), calls=%async_computation.8 | async-start | bytes 2621440 | tf_op jit(solution)/shard_map/reduce_scatter | solution.py:102
  240.6 187.3 %copy-start.6 = (bf16[512,2048]{1,0:T(8,128)(2,1)S(1)}, bf16[512,2048]{1,0:T(8,128)(2,1)}, u32[]{:S(2)}) copy-start(bf16[512,2048]{1,0:T(8,128)(2,1)} %all-gather.8.cloned.1.call-done) | copy-start | bytes 6291460
  428.0 15.6 %copy-start.5 = (bf16[2048]{0:T(1024)(128)(2,1)S(1)}, bf16[2048]{0:T(1024)(128)(2,1)}, u32[]{:S(2)}) copy-start(bf16[2048]{0:T(1024)(128)(2,1)} %param.23) | copy-start | bytes 12292
Sparse Core Ops, SparseCore 0:
  12.2 25.2 all-gather.5
  122.8 32.3 reduce-scatter.2
  443.6 29.3 reduce-scatter.4
Sparse Core Ops, SparseCore 1:
  125.3 93.2 all-gather.9
  220.0 20.5 all-gather.7
  242.7 92.1 all-gather.11
  336.9 91.0 all-gather.13
where the time goes:
time: 486 us; the launch traced here: 485 us
  waiting for transfers between devices  320 us (66%)
  blocking collectives  102 us (21%)
  matrix products  31.6 us (7%)
  other arithmetic  16 us (3%)
  between operations  15 us (3%)
    all_gather x1, waiting for transfers between devices, shards(): whole_down = lax.all_gather(ffn_down, 'fs', axis=1, tiled=True)  93.1 us
    all_gather x1, waiting for transfers between devices, shards(): lax.all_gather(ffn_value, 'fs', axis=0, tiled=True)  85.8 us
    all_gather x1, waiting for transfers between devices, shards(): lax.all_gather(ffn_gate, 'fs', axis=0, tiled=True)  56.3 us
    all_gather x1, blocking collectives, shards(): lax.all_gather(signal_proj, 'fs', axis=0, tiled=True)  33.3 us
    reduce_scatter x1, waiting for transfers between devices, shards(): lax.psum_scatter(jnp.dot(selected, out_columns, preferred_element_type=jn...  31.8 us
    all_gather x1, blocking collectives, shards(): lax.all_gather(gate_proj, 'fs', axis=0, tiled=True)  31.5 us
    all_gather x1, blocking collectives, shards(): out_columns = lax.all_gather(mixer_out, 'fs', axis=1, tiled=True)  31.2 us
    reduce_scatter x1, waiting for transfers between devices, shards(): lax.psum_scatter(jnp.dot(selected, whole_down, preferred_element_type=jnp...  29.5 us
  transfers between devices with their start and end apart: 7, of which 6 were waited for; matrix products, arithmetic and copies ran while one was open for 3% of the time, Pallas kernels for 0%

commit v1 on v0

--- a/solution.py
+++ b/solution.py
@@ -10,6 +10,20 @@
 SEGMENT = 64
 EPSILON = 1e-05
 RESIDUAL_SCALE = math.sqrt(2.0)
+
+
+def _list_state(work_x):
+    n_lanes = lax.axis_size("fs")
+    tile_out = work_x
+    blocks_here = [tile_out]
+    k0 = 1
+    v_next = sorted(((dd, (dd + 1) % n_lanes) for dd in range(n_lanes)))
+    while k0 < n_lanes:
+        tile_out = lax.ppermute(tile_out, "fs", v_next)
+        blocks_here.insert(0, tile_out)
+        k0 += 1
+    inter = jnp.concatenate(blocks_here, axis=1)
+    return jnp.roll(inter, (lax.axis_index("fs") + 1) * work_x.shape[1], 1)
 
 
 def normalize(values):
@@ -96,7 +110,7 @@
     left_part = group_ffn
     gate_pre = jnp.dot(left_part, pieces[0], preferred_element_type=jnp.float32)
     value_pre = jnp.dot(left_part, pieces[1], preferred_element_type=jnp.float32)
-    whole_down = lax.all_gather(ffn_down, "fs", axis=1, tiled=True)
+    whole_down = _list_state(ffn_down)
     hidden = (jax.nn.silu(causal_conv(gate_pre, conv_taps)) * value_pre).astype(jnp.bfloat16)
     selected = hidden
     ffn_out = lax.psum_scatter(

time: 486 us -> 458 us (0.942)
  waiting for transfers between devices: 320 us -> 267 us
  local copies, waits for them, and re-layouts: 0.08 us -> 23 us
    ppermute x0 -> x7, waiting for transfers between devices: none -> 202 us  [_list_state(): tile_out = lax.ppermute(tile_out, 'fs', v_next)]
    all_gather x1 -> x0, waiting for transfers between devices: 93.1 us -> none  [shards(): whole_down = lax.all_gather(ffn_down, 'fs', axis=1, tiled=True)]
    all_gather x1, waiting for transfers between devices: 85.8 us -> 1.99 us  [shards(): lax.all_gather(ffn_value, 'fs', axis=0, tiled=True)]
    all_gather x1, waiting for transfers between devices: 56.3 us -> 0.01 us  [shards(): lax.all_gather(ffn_gate, 'fs', axis=0, tiled=True)]
    all_gather x1, waiting for transfers between devices: 22 us -> 0.01 us  [shards(): group_ffn = lax.all_gather(ffn_input, 'tp', axis=0, tiled=True)]
    unnamed x14 -> x35, local copies, waits for them, and re-layouts: 0.03 us -> 22 us
  transfers between devices with their start and end apart: 7 -> 13, of which waited for: 6 -> 10; matrix products, arithmetic and copies ran while one was open for 3% -> 8% of each run, Pallas kernels for 0% -> 0%
where the time goes in v1:
time: 458 us; the launch traced here: 457 us
  waiting for transfers between devices  267 us (58%)
  blocking collectives  102 us (22%)
  matrix products  32 us (7%)
  local copies, waits for them, and re-layouts  23 us (5%)
  other arithmetic  16 us (3%)
  between operations  14.9 us (3%)
    ppermute x7, waiting for transfers between devices, _list_state(): tile_out = lax.ppermute(tile_out, 'fs', v_next)  202 us
    all_gather x1, blocking collectives, shards(): lax.all_gather(signal_proj, 'fs', axis=0, tiled=True)  33.3 us
    reduce_scatter x1, waiting for transfers between devices, shards(): lax.psum_scatter(jnp.dot(selected, out_columns, preferred_element_type=jn...  32 us
    all_gather x1, blocking collectives, shards(): lax.all_gather(gate_proj, 'fs', axis=0, tiled=True)  31.5 us
    all_gather x1, blocking collectives, shards(): out_columns = lax.all_gather(mixer_out, 'fs', axis=1, tiled=True)  31.5 us
    reduce_scatter x1, waiting for transfers between devices, shards(): lax.psum_scatter(jnp.dot(selected, whole_down, preferred_element_type=jnp...  30.2 us
    unnamed x35, local copies, waits for them, and re-layouts  22 us
    dot_general x1, matrix products, shards(): jnp.dot(selected, whole_down, preferred_element_type=jnp.float32)  15.7 us
  transfers between devices with their start and end apart: 13, of which 10 were waited for; matrix products, arithmetic and copies ran while one was open for 8% of the time, Pallas kernels for 0%

profile of v1, /device:TPU:0, one launch (start us, length us, event | category | flops | bytes accessed | tf_op | source)
XLA Modules:
  0.0 457.4 jit_solution(10864396581177287229)
XLA Ops:
  8.6 1.3 fusion.12
  9.9 2.2 fusion.13
  12.9 33.3 %all_gather.23 = bf16[2048,128]{1,0:T(8,128)(2,1)S(1)} all-gather(bf16[256,128]{1,0:T(8,128)(2,1)} %param.14), channel_id=1, replica_groups=mesh['fs'=8,'tp'=4] {'fs'}, dimensions={0}, use_global_device_ids=true | all-gather | bytes 589824 | tf_op jit(solution)/shard_map/all_gather | solution.py:68
  46.2 31.5 %all_gather.22 = bf16[2048,128]{1,0:T(8,128)(2,1)S(1)} all-gather(bf16[256,128]{1,0:T(8,128)(2,1)} %param.13), channel_id=1, replica_groups=mesh['fs'=8,'tp'=4] {'fs'}, dimensions={0}, use_global_device_ids=true | all-gather | bytes 589824 | tf_op jit(solution)/shard_map/all_gather | solution.py:67
  77.7 31.5 %all_gather.24 = bf16[128,2048]{1,0:T(8,128)(2,1)S(1)} all-gather(bf16[128,256]{1,0:T(8,128)(2,1)} %param.17), channel_id=1, replica_groups=mesh['fs'=8,'tp'=4] {'fs'}, dimensions={1}, use_global_device_ids=true | all-gather | bytes 589824 | tf_op jit(solution)/shard_map/all_gather | solution.py:92
  109.3 2.5 fusion.44
  111.8 5.7 %all-reduce.2 = (f32[512]{0:T(512)S(1)}, f32[512]{0:T(512)S(1)}) all-reduce(f32[512]{0:T(512)S(1)} %get-tuple-element.6, f32[512]{0:T(512)S(1)} %get-tuple-element.5), channel_id=1, replica_groups=mesh['fs'=8,'tp'=4] {'tp'}, use_global_device_ids=true, to_apply=%region_5.6 | all-reduce | flops 1024 | bytes 8192 | tf_op jit(solution)/shard_map/psum | solution.py:75
  118.6 2.3 fusion.26
  120.9 2.0 convolution_convert_fusion
  123.7 32.0 %reduce-scatter.3.cloned.1.call-done = bf16[128,2048]{1,0:T(8,128)(2,1)} async-done(((bf16[512,2048]{1,0:T(8,128)(2,1)}), bf16[128,2048]{1,0:T(8,128)(2,1)}) %reduce-scatter.3.cloned.1.call-update) | async-done | bytes 524304 | tf_op jit(solution)/shard_map/reduce_scatter | solution.py:94
  155.7 1.3 fusion.17
  157.0 1.4 multiply_reduce_fusion.1
  158.4 1.4 convert_reduce_fusion
  161.9 1.5 collective-permute-start
  163.4 30.7 %collective-permute-done = bf16[1408,256]{1,0:T(8,128)(2,1)S(1)} collective-permute-done((bf16[1408,256]{1,0:T(8,128)(2,1)S(1)}, bf16[1408,256]{1,0:T(8,128)(2,1)S(1)}, u32[]{:S(2)}, u32[]{:S(2)}) %collective-permute-start) | collective-permute-done | bytes 720928 | tf_op jit(solution)/shard_map/ppermute | solution.py:22
  194.3 35.4 %collective-permute-done.1 = bf16[1408,256]{1,0:T(8,128)(2,1)S(1)} collective-permute-done((bf16[1408,256]{1,0:T(8,128)(2,1)S(1)}, bf16[1408,256]{1,0:T(8,128)(2,1)S(1)}, u32[]{:S(2)}, u32[]{:S(2)}) %collective-permute-start.1) | collective-permute-done | bytes 720928 | tf_op jit(solution)/shard_map/ppermute | solution.py:22
  229.7 30.0 %collective-permute-done.2 = bf16[1408,256]{1,0:T(8,128)(2,1)S(1)} collective-permute-done((bf16[1408,256]{1,0:T(8,128)(2,1)S(1)}, bf16[1408,256]{1,0:T(8,128)(2,1)S(1)}, u32[]{:S(2)}, u32[]{:S(2)}) %collective-permute-start.2) | collective-permute-done | bytes 720928 | tf_op jit(solution)/shard_map/ppermute | solution.py:22
  260.6 19.1 %collective-permute-done.3 = bf16[1408,256]{1,0:T(8,128)(2,1)S(1)} collective-permute-done((bf16[1408,256]{1,0:T(8,128)(2,1)S(1)}, bf16[1408,256]{1,0:T(8,128)(2,1)S(1)}, u32[]{:S(2)}, u32[]{:S(2)}) %collective-permute-start.3) | collective-permute-done | bytes 720928 | tf_op jit(solution)/shard_map/ppermute | solution.py:22
  279.6 23.8 %collective-permute-done.4 = bf16[1408,256]{1,0:T(8,128)(2,1)S(1)} collective-permute-done((bf16[1408,256]{1,0:T(8,128)(2,1)S(1)}, bf16[1408,256]{1,0:T(8,128)(2,1)S(1)}, u32[]{:S(2)}, u32[]{:S(2)}) %collective-permute-start.4) | collective-permute-done | bytes 720928 | tf_op jit(solution)/shard_map/ppermute | solution.py:22
  304.3 33.5 %collective-permute-done.5 = bf16[1408,256]{1,0:T(8,128)(2,1)} collective-permute-done((bf16[1408,256]{1,0:T(8,128)(2,1)S(1)}, bf16[1408,256]{1,0:T(8,128)(2,1)}, u32[]{:S(2)}, u32[]{:S(2)}) %collective-permute-start.5) | collective-permute-done | bytes 720928 | tf_op jit(solution)/shard_map/ppermute | solution.py:22
  337.9 29.7 %collective-permute-done.6 = bf16[1408,256]{1,0:T(8,128)(2,1)} collective-permute-done((bf16[1408,256]{1,0:T(8,128)(2,1)}, bf16[1408,256]{1,0:T(8,128)(2,1)}, u32[]{:S(2)}, u32[]{:S(2)}) %collective-permute-start.6) | collective-permute-done | bytes 720928 | tf_op jit(solution)/shard_map/ppermute | solution.py:22
  367.6 2.1 constant_dynamic-update-slice_fusion.15
  369.8 2.1 constant_dynamic-update-slice_fusion.14
  371.8 2.1 constant_dynamic-update-slice_fusion.13
  378.8 2.1 constant_dynamic-update-slice_fusion.7
  380.9 2.1 constant_dynamic-update-slice_fusion.6
  388.8 8.5 %fusion.45 = f32[512,1408]{1,0:T(8,128)} fusion(bf16[512,2048]{1,0:T(8,128)(2,1)} %all-gather.7.cloned.1.call-done, bf16[2048,1408]{1,0:T(8,128)(2,1)} %all-gather.9.cloned.1.call-done), kind=kOutput, calls=%fused_computation.93 | convolution fusion | flops 2952790016 | bytes 10747904 | tf_op jit(solution)/shard_map/dot_general | solution.py:111
  397.3 2.0 all-gather.11.cloned.1.call-done
  399.3 15.7 %fusion.3 = bf16[512,2048]{1,0:T(8,128)(2,1)} fusion(bf16[1408,4096]{1,0:T(8,128)(2,1)} %constant_dynamic-update-slice_fusion, s32[]{:T(128)S(6)} %select_n.43, bf16[512,2048]{1,0:T(8,128)(2,1)S(1)} %copy-done.9, bf16[2048,1408]{1,0:T(8,128)(2,1)} %all-gather.11.cloned.1.call-done, f32[512,1408]{1,0:T(8,128)} %fusion.45, f32[511,1408]{1,0:T(8,128)} %bitcast.23, ...), kind=kOutput, calls=%fused_computation.5 | convolution fusion | flops 5914558464 | bytes 24396292 | tf_op jit(solution)/shard_map/dot_general | solution.py:117
  415.1 30.2 %reduce-scatter.5.cloned.1.call-done = bf16[128,2048]{1,0:T(8,128)(2,1)} async-done(((bf16[512,2048]{1,0:T(8,128)(2,1)}), bf16[128,2048]{1,0:T(8,128)(2,1)}) %reduce-scatter.5.cloned.1.call-update) | async-done | bytes 524304 | tf_op jit(solution)/shard_map/reduce_scatter | solution.py:116
  446.6 1.4 multiply_reduce_fusion
  448.0 2.1 multiply_convert_fusion
  (74 shorter events, 20.0 us)
Async XLA Ops:
  7.4 101.9 %all-gather.5.cloned.1.call-start = ((), (), s32[]{:S(2)}) async-start(), calls=%async_computation.2 | async-start | bytes 2621440 | tf_op jit(solution)/shard_map/all_gather | solution.py:63
  12.1 143.6 %reduce-scatter.3.cloned.1.call-start = ((), (), s32[]{:S(2)}) async-start(), calls=%async_computation.3 | async-start | bytes 2621440 | tf_op jit(solution)/shard_map/reduce_scatter | solution.py:94
  109.3 14.4 %copy-start.7 = (bf16[2048]{0:T(1024)(128)(2,1)S(1)}, bf16[2048]{0:T(1024)(128)(2,1)}, u32[]{:S(2)}) copy-start(bf16[2048]{0:T(1024)(128)(2,1)} %param.18) | copy-start | bytes 12292
  109.3 46.4 %copy-start = (bf16[128,2048]{1,0:T(8,128)(2,1)S(1)}, bf16[128,2048]{1,0:T(8,128)(2,1)}, u32[]{:S(2)}) copy-start(bf16[128,2048]{1,0:T(8,128)(2,1)} %param.12) | copy-start | bytes 1572868
  120.9 41.0 %copy-start.1 = (bf16[1408,256]{1,0:T(8,128)(2,1)S(1)}, bf16[1408,256]{1,0:T(8,128)(2,1)}, u32[]{:S(2)}) copy-start(bf16[1408,256]{1,0:T(8,128)(2,1)} %param.22) | copy-start | bytes 2162692
  120.9 216.9 %copy-start.6 = (bf16[3,1408]{1,0:T(4,128)(2,1)S(1)}, bf16[3,1408]{1,0:T(4,128)(2,1)}, u32[]{:S(2)}) copy-start(bf16[3,1408]{1,0:T(4,128)(2,1)} %param.21) | copy-start | bytes 25348
  123.0 265.8 %all-gather.9.cloned.1.call-start = ((), (), s32[]{:S(2)}) async-start(), calls=%async_computation.5 | async-start | bytes 6488064 | tf_op jit(solution)/shard_map/all_gather | solution.py:107
  123.6 265.3 %all-gather.7.cloned.1.call-start = ((), (), s32[]{:S(2)}) async-start(), calls=%async_computation.4 | async-start | bytes 2621440 | tf_op jit(solution)/shard_map/all_gather | solution.py:105
  161.2 238.1 %all-gather.11.cloned.1.call-start = ((), (), s32[]{:S(2)}) async-start(), calls=%async_computation.6 | async-start | bytes 6488064 | tf_op jit(solution)/shard_map/all_gather | solution.py:108
  161.8 283.5 %reduce-scatter.5.cloned.1.call-start = ((), (), s32[]{:S(2)}) async-start(), calls=%async_computation.7 | async-start | bytes 2621440 | tf_op jit(solution)/shard_map/reduce_scatter | solution.py:116
  161.9 32.2 %collective-permute-start = (bf16[1408,256]{1,0:T(8,128)(2,1)S(1)}, bf16[1408,256]{1,0:T(8,128)(2,1)S(1)}, u32[]{:S(2)}, u32[]{:S(2)}) collective-permute-start(bf16[1408,256]{1,0:T(8,128)(2,1)S(1)} %copy-done.1), channel_id=1, source_target_pairs={{0,4},{4,8},{8,12},{12,16},{16,20},{20,24},{24,28},{28,0},{1,5},{5... | collective-permute-start | bytes 2162696 | tf_op jit(solution)/shard_map/ppermute | solution.py:22
  194.1 35.6 %collective-permute-start.1 = (bf16[1408,256]{1,0:T(8,128)(2,1)S(1)}, bf16[1408,256]{1,0:T(8,128)(2,1)S(1)}, u32[]{:S(2)}, u32[]{:S(2)}) collective-permute-start(bf16[1408,256]{1,0:T(8,128)(2,1)S(1)} %collective-permute-done), channel_id=1, source_target_pairs={{0,4},{4,8},{8,12},{12,16},{16,20},{20,24},{24,28},{28,0},{1,5},{5... | collective-permute-start | bytes 2162696 | tf_op jit(solution)/shard_map/ppermute | solution.py:22
  229.7 30.0 %collective-permute-start.2 = (bf16[1408,256]{1,0:T(8,128)(2,1)S(1)}, bf16[1408,256]{1,0:T(8,128)(2,1)S(1)}, u32[]{:S(2)}, u32[]{:S(2)}) collective-permute-start(bf16[1408,256]{1,0:T(8,128)(2,1)S(1)} %collective-permute-done.1), channel_id=1, source_target_pairs={{0,4},{4,8},{8,12},{12,16},{16,20},{20,24},{24,28},{28,0},{1,5},{5... | collective-permute-start | bytes 2162696 | tf_op jit(solution)/shard_map/ppermute | solution.py:22
  259.7 0.9 copy-start.2
  260.6 19.1 %collective-permute-start.3 = (bf16[1408,256]{1,0:T(8,128)(2,1)S(1)}, bf16[1408,256]{1,0:T(8,128)(2,1)S(1)}, u32[]{:S(2)}, u32[]{:S(2)}) collective-permute-start(bf16[1408,256]{1,0:T(8,128)(2,1)S(1)} %collective-permute-done.2), channel_id=1, source_target_pairs={{0,4},{4,8},{8,12},{12,16},{16,20},{20,24},{24,28},{28,0},{1,5},{5... | collective-permute-start | bytes 2162696 | tf_op jit(solution)/shard_map/ppermute | solution.py:22
  279.6 23.8 %collective-permute-start.4 = (bf16[1408,256]{1,0:T(8,128)(2,1)S(1)}, bf16[1408,256]{1,0:T(8,128)(2,1)S(1)}, u32[]{:S(2)}, u32[]{:S(2)}) collective-permute-start(bf16[1408,256]{1,0:T(8,128)(2,1)S(1)} %collective-permute-done.3), channel_id=1, source_target_pairs={{0,4},{4,8},{8,12},{12,16},{16,20},{20,24},{24,28},{28,0},{1,5},{5... | collective-permute-start | bytes 2162696 | tf_op jit(solution)/shard_map/ppermute | solution.py:22
  303.4 0.9 copy-start.4
  304.3 33.5 %collective-permute-start.5 = (bf16[1408,256]{1,0:T(8,128)(2,1)S(1)}, bf16[1408,256]{1,0:T(8,128)(2,1)}, u32[]{:S(2)}, u32[]{:S(2)}) collective-permute-start(bf16[1408,256]{1,0:T(8,128)(2,1)S(1)} %collective-permute-done.4), channel_id=1, source_target_pairs={{0,4},{4,8},{8,12},{12,16},{16,20},{20,24},{24,28},{28,0},{1,5},{5... | collective-permute-start | bytes 2162696 | tf_op jit(solution)/shard_map/ppermute | solution.py:22
  337.8 29.8 %collective-permute-start.6 = (bf16[1408,256]{1,0:T(8,128)(2,1)}, bf16[1408,256]{1,0:T(8,128)(2,1)}, u32[]{:S(2)}, u32[]{:S(2)}) collective-permute-start(bf16[1408,256]{1,0:T(8,128)(2,1)} %collective-permute-done.5), channel_id=1, source_target_pairs={{0,4},{4,8},{8,12},{12,16},{16,20},{20,24},{24,28},{28,0},{1,5},{5... | collective-permute-start | bytes 2162696 | tf_op jit(solution)/shard_map/ppermute | solution.py:22
  337.8 37.2 %copy-start.3 = (bf16[1408,256]{1,0:T(8,128)(2,1)S(1)}, bf16[1408,256]{1,0:T(8,128)(2,1)}, u32[]{:S(2)}) copy-start(bf16[1408,256]{1,0:T(8,128)(2,1)} %copy-done.2) | copy-start | bytes 2162692
  371.8 11.2 %copy-start.5 = (bf16[1408,256]{1,0:T(8,128)(2,1)S(1)}, bf16[1408,256]{1,0:T(8,128)(2,1)}, u32[]{:S(2)}) copy-start(bf16[1408,256]{1,0:T(8,128)(2,1)} %copy-done.4) | copy-start | bytes 2162692
  388.8 10.5 %copy-start.9 = (bf16[512,2048]{1,0:T(8,128)(2,1)S(1)}, bf16[512,2048]{1,0:T(8,128)(2,1)}, u32[]{:S(2)}) copy-start(bf16[512,2048]{1,0:T(8,128)(2,1)} %all-gather.7.cloned.1.call-done) | copy-start | bytes 6291460
  399.3 15.8 %copy-start.8 = (bf16[2048]{0:T(1024)(128)(2,1)S(1)}, bf16[2048]{0:T(1024)(128)(2,1)}, u32[]{:S(2)}) copy-start(bf16[2048]{0:T(1024)(128)(2,1)} %param.23) | copy-start | bytes 12292
Sparse Core Ops, SparseCore 0:
  12.2 25.2 all-gather.4
  123.1 32.5 reduce-scatter.2
  415.2 30.0 reduce-scatter.4
Sparse Core Ops, SparseCore 1:
  125.7 118.8 all-gather.8
  246.0 33.3 all-gather.6
  281.4 117.8 all-gather.10
